TPU v7x, 32 devices: a whole 2x2x4 slice. The times are simulated.
32 devices in a mesh: sp: 4 (over y, core), tp: 8 (over z, x).
Axes of the slice: x: 2, y: 2, z: 4, core: 2. Of those that a mesh axis runs over, the one named last changes fastest.
Arguments:
- queries: bfloat16 [512, 3072], P('sp'), may hold values from -6 to 6
- attn_out: bfloat16 [512, 3072], P('sp'), may hold values from -3 to 3
- log_norm: float32 [512, 12], P('sp'), as said below
- cotangent: bfloat16 [512, 3072], P('sp'), may hold values from -96 to 96
- keys: bfloat16 [1024, 512], P(('sp', 'tp')), may hold values from -6 to 6
- values: bfloat16 [1024, 512], P(('sp', 'tp')), may hold values from -6 to 6
- source: bfloat16 [1024, 3072], P('sp', 'tp'), may hold values from -6 to 6
- w_query: bfloat16 [3072, 3072], P('tp'), may hold values from -0.109375 to 0.109375
- w_key: bfloat16 [3072, 512], P('tp'), may hold values from -0.109375 to 0.109375
- w_value: bfloat16 [3072, 512], P('tp'), may hold values from -0.109375 to 0.109375
Outputs:
- d_target: bfloat16 [512, 3072], P('sp', 'tp')
- d_source: bfloat16 [1024, 3072], P('sp', 'tp')
- d_wvalue: float32 [3072, 512], P('tp')
Inputs may be any that keep to these rules, and one draw needn't show every extreme that they name: `log_norm`: the logarithm of the softmax total saved by the forward pass, near log(1024) + 0.5.
All inputs are finite; a program needn't handle non-finite values.
Results may differ from a plain program's by a relative error of at most 0.024.
Values may be sent and summed in bfloat16 or wider, within the bound.
A program may use at most 64 MiB of HBM per device.

v0:
```python
import math

import jax
import jax.numpy as jnp
from jax import lax
from jax.sharding import PartitionSpec as P

HEADS = 12
KV_HEADS = 2
HEAD_DIM = 256


def shards(queries, attn_out, log_norm, cotangent, keys, values, source, w_query, w_key, w_value):
    single_precision = jnp.float32
    repeat = HEADS // KV_HEADS
    score_scale = 1.0 / math.sqrt(HEAD_DIM)
    rows = queries.shape[0]
    near_keys, near_values = (
        lax.all_gather(keys, "sp", axis=0, tiled=True),
        lax.all_gather(values, "sp", axis=0, tiled=True),
    )
    span = near_keys.shape[0]
    query_tensor4 = queries.reshape(rows, KV_HEADS, repeat, HEAD_DIM)
    output_gradient4 = cotangent.reshape(rows, KV_HEADS, repeat, HEAD_DIM)
    out4 = attn_out.reshape(rows, KV_HEADS, repeat, HEAD_DIM)
    shared_key_heads = near_keys.reshape(span, KV_HEADS, HEAD_DIM)
    shared_value_heads = near_values.reshape(span, KV_HEADS, HEAD_DIM)
    delta = jnp.sum(
        output_gradient4.astype(single_precision) * out4.astype(single_precision), axis=3
    )
    delta = jnp.transpose(delta, (1, 2, 0))[..., None]
    lse = jnp.transpose(log_norm.reshape(rows, KV_HEADS, repeat), (1, 2, 0))[..., None]
    logit_scores = (
        jnp.einsum(
            "znjk,wnk->njzw",
            query_tensor4,
            shared_key_heads,
            preferred_element_type=single_precision,
        )
        * score_scale
    )
    probs = jnp.exp(logit_scores - lse)
    probabilities16 = probs.astype(jnp.bfloat16)
    prob_gradient = jnp.einsum(
        "znjk,wnk->njzw",
        output_gradient4,
        shared_value_heads,
        preferred_element_type=single_precision,
    )
    score_gradient = (probs * (prob_gradient - delta)).astype(jnp.bfloat16)
    query_gradient_piece = (
        jnp.einsum(
            "wohn,nwb->hwob",
            score_gradient,
            shared_key_heads,
            preferred_element_type=single_precision,
        )
        * score_scale
    )
    query_gradient_piece = query_gradient_piece.reshape(rows, -1)
    key_gradient_piece = (
        jnp.einsum(
            "nkjv,jnka->vna", score_gradient, query_tensor4, preferred_element_type=single_precision
        )
        * score_scale
    )
    value_gradient_piece = jnp.einsum(
        "nkjv,jnka->vna", probabilities16, output_gradient4, preferred_element_type=single_precision
    )
    own_keys, own_values = (
        lax.psum_scatter(
            key_gradient_piece.reshape(span, -1).astype(jnp.bfloat16),
            "sp",
            scatter_dimension=0,
            tiled=True,
        ).astype(jnp.float32),
        lax.psum_scatter(
            value_gradient_piece.reshape(span, -1).astype(jnp.bfloat16),
            "sp",
            scatter_dimension=0,
            tiled=True,
        ).astype(jnp.float32),
    )
    stacked = jnp.concatenate(
        [own_keys.astype(jnp.bfloat16), own_values.astype(jnp.bfloat16)], axis=1
    )
    group = lax.all_gather(stacked, "tp", axis=0, tiled=True)
    weights = jnp.concatenate([w_key, w_value], axis=1)
    d_source = lax.dot_general(
        group, weights, (((1,), (1,)), ((), ())), preferred_element_type=single_precision
    ).astype(jnp.bfloat16)
    kv_width = w_value.shape[1]
    weight_term = lax.dot_general(
        source,
        group[:, kv_width:],
        (((0,), (0,)), ((), ())),
        preferred_element_type=single_precision,
    )
    d_wvalue = lax.psum(weight_term.astype(jnp.bfloat16), "sp").astype(jnp.float32)
    dq16 = lax.psum(query_gradient_piece, "tp").astype(jnp.bfloat16)
    d_target = lax.dot_general(
        dq16, w_query, (((1,), (1,)), ((), ())), preferred_element_type=single_precision
    ).astype(jnp.bfloat16)
    return (d_target, d_source, d_wvalue)


def solution(mesh):
    in_specs = (
        P("sp", None),
        P("sp", None),
        P("sp", None),
        P("sp", None),
        P(("sp", "tp"), None),
        P(("sp", "tp"), None),
        P("sp", "tp"),
        P("tp", None),
        P("tp", None),
        P("tp", None),
    )
    out_specs = (P("sp", "tp"), P("sp", "tp"), P("tp", None))
    return jax.shard_map(shards, mesh=mesh, in_specs=in_specs, out_specs=out_specs, check_vma=False)
```

profile of v0, /device:TPU:0, one launch (start us, length us, event | category | flops | bytes accessed | tf_op | source)
XLA Modules:
  0.0 197.1 jit_solution(18364416684558412824)
XLA Ops:
  7.2 0.0 reduce-scatter.9.cloned.1.call-start
  7.2 0.8 reshape.35
  8.1 6.7 %all_gather.9 = bf16[128,512]{1,0:T(8,128)(2,1)S(1)} all-gather(bf16[32,512]{1,0:T(8,128)(2,1)} %param.14), channel_id=1, replica_groups=mesh['sp'=4,'tp'=8] {'sp'}, dimensions={0}, use_global_device_ids=true | all-gather | bytes 163840 | tf_op jit(solution)/shard_map/all_gather | solution.py:19
  14.8 0.1 copy.36
  14.9 2.3 %copy.37 = bf16[128,3072]{0,1:T(8,128)(2,1)} copy(bf16[128,3072]{1,0:T(8,128)(2,1)} %param.10) | data formatting | bytes 1572864 | tf_op args[0]
  17.3 1.5 copy.41
  18.8 1.5 fusion.4
  20.3 0.9 copy-done.2
  21.2 0.4 fusion.11
  21.5 0.1 copy.51
  21.7 0.8 copy.73
  22.5 0.0 reduce-scatter.7.cloned.1.call-start
  22.5 5.6 %all_gather.10 = bf16[128,512]{1,0:T(8,128)(2,1)S(1)} all-gather(bf16[32,512]{1,0:T(8,128)(2,1)S(1)} %copy-done.8), channel_id=1, replica_groups=mesh['sp'=4,'tp'=8] {'sp'}, dimensions={0}, use_global_device_ids=true | all-gather | bytes 163840 | tf_op jit(solution)/shard_map/all_gather | solution.py:20
  28.1 0.8 copy.40
  28.9 2.3 %copy.44 = bf16[128,3072]{0,1:T(8,128)(2,1)} copy(bf16[128,3072]{1,0:T(8,128)(2,1)} %param.11) | data formatting | bytes 1572864 | tf_op args[1]
  31.2 1.5 fusion
  32.7 0.3 fusion.6
  33.0 0.4 fusion.12
  33.4 0.1 copy.49
  33.5 0.8 copy.71
  34.3 0.0 reduce-scatter.7.cloned.1.call-update
  34.3 0.0 all-reduce.3.cloned.1.call-start
  34.4 1.6 multiply_bitcast_fusion
  36.0 3.0 %copy.47 = f32[128,2,6,256]{0,3,2,1:T(8,128)} copy(f32[128,2,6,256]{3,0,2,1:T(8,128)} %multiply_bitcast_fusion) | data formatting | bytes 3145728 | tf_op jit(solution)/shard_map/mul | solution.py:52
  39.0 80.8 %all-reduce.4 = bf16[128,3072]{0,1:T(8,128)(2,1)S(1)} all-reduce(f32[128,3072]{0,1:T(8,128)} %bitcast.80), channel_id=1, replica_groups=mesh['sp'=4,'tp'=8] {'tp'}, use_global_device_ids=true, to_apply=%region_1.0 | all-reduce | flops 393216 | bytes 2359296 | tf_op jit(solution)/shard_map/psum | solution.py:100
  119.9 1.5 convolution_convert_fusion.2
  121.4 0.8 pad_maximum_fusion
  122.1 31.5 %all_gather.11 = bf16[256,1024]{1,0:T(8,128)(2,1)S(1)} all-gather(bf16[32,1024]{1,0:T(8,128)(2,1)S(1)} %pad_maximum_fusion), channel_id=1, replica_groups=mesh['sp'=4,'tp'=8] {'tp'}, dimensions={0}, use_global_device_ids=true | all-gather | bytes 589824 | tf_op jit(solution)/shard_map/all_gather | solution.py:87
  153.6 1.1 fusion.7
  154.7 2.3 %convolution_convert_fusion.1 = bf16[256,384]{1,0:T(8,128)(2,1)} fusion(bf16[256,1024]{1,0:T(8,128)(2,1)S(1)} %all_gather.11, bf16[384,512]{1,0:T(8,128)(2,1)} %param.19, bf16[384,512]{1,0:T(8,128)(2,1)} %param.18), kind=kOutput, calls=%fused_computation.13 | convolution fusion | flops 202997760 | bytes 1507328 | tf_op jit(solution)/shard_map/dot_general | solution.py:89
  157.0 31.5 %all-reduce.3.cloned.1.call-done = bf16[384,512]{0,1:T(8,128)(2,1)} async-done(((bf16[384,512]{0,1:T(8,128)(2,1)}), bf16[384,512]{0,1:T(8,128)(2,1)}) %all-reduce.3.cloned.1.call-update) | async-done | bytes 393232 | tf_op jit(solution)/shard_map/psum | solution.py:99
  188.5 2.0 %copy.54 = f32[384,512]{1,0:T(8,128)} copy(bf16[384,512]{0,1:T(8,128)(2,1)} %all-reduce.3.cloned.1.call-done) | data formatting | bytes 1179648
  (21 shorter events, 0.1 us)
Async XLA Ops:
  7.2 112.7 %copy-start = (bf16[384,3072]{1,0:T(8,128)(2,1)S(1)}, bf16[384,3072]{1,0:T(8,128)(2,1)}, u32[]{:S(2)}) copy-start(bf16[384,3072]{1,0:T(8,128)(2,1)} %param.17) | copy-start | bytes 7077892
  7.2 114.2 %reduce-scatter.9.cloned.1.call-start = ((), (), s32[]{:S(2)}) async-start(), calls=%async_computation.4 | async-start | bytes 163840 | tf_op jit(solution)/shard_map/reduce_scatter | solution.py:77
  14.9 3.9 %copy-start.4 = (bf16[128,512]{0,1:T(8,128)(2,1)}, bf16[128,512]{0,1:T(8,128)(2,1)S(1)}, u32[]{:S(2)}) copy-start(bf16[128,512]{0,1:T(8,128)(2,1)S(1)} %copy.36) | copy-start | bytes 393220
  20.3 0.9 copy-start.2
  20.3 2.2 %copy-start.8 = (bf16[32,512]{1,0:T(8,128)(2,1)S(1)}, bf16[32,512]{1,0:T(8,128)(2,1)}, u32[]{:S(2)}) copy-start(bf16[32,512]{1,0:T(8,128)(2,1)} %param.15) | copy-start | bytes 98308
  22.5 98.9 %reduce-scatter.7.cloned.1.call-start = ((), (), s32[]{:S(2)}) async-start(), calls=%async_computation.3 | async-start | bytes 163840 | tf_op jit(solution)/shard_map/reduce_scatter | solution.py:71
  31.2 1.5 copy-start.3
  31.2 1.5 copy-start.6
  31.2 1.8 copy-start.1
  33.0 1.4 copy-start.5
  34.3 154.2 %all-reduce.3.cloned.1.call-start = ((), (), s32[]{:S(2)}) async-start(), calls=%async_computation.2 | async-start | bytes 786432 | tf_op jit(solution)/shard_map/psum | solution.py:99
  119.9 33.8 %copy-start.7 = (bf16[256,384]{1,0:T(8,128)(2,1)S(1)}, bf16[256,384]{1,0:T(8,128)(2,1)}, u32[]{:S(2)}) copy-start(bf16[256,384]{1,0:T(8,128)(2,1)} %param.16) | copy-start | bytes 589828
Sparse Core Ops, SparseCore 0:
  22.6 21.2 reduce-scatter.8
  46.9 19.6 reduce-scatter.6
  154.9 33.6 all-reduce.2
where the time goes:
time: 198 us; the launch traced here: 197 us
  blocking collectives  125 us (63%)
  waiting for transfers between devices  31.6 us (16%)
  local copies, waits for them, and re-layouts  15.6 us (8%)
  between operations  13.9 us (7%)
  matrix products  8.94 us (5%)
  other arithmetic  2.26 us (1%)
    psum x1, blocking collectives, shards(): dq16 = lax.psum(query_gradient_piece, 'tp').astype(jnp.bfloat16)  80.8 us
    psum x1, waiting for transfers between devices, shards(): lax.psum(weight_term.astype(jnp.bfloat16), 'sp').astype(jnp.float32)  31.5 us
    all_gather x1, blocking collectives, shards(): group = lax.all_gather(stacked, 'tp', axis=0, tiled=True)  31.5 us
    unnamed x24, local copies, waits for them, and re-layouts  10.6 us
    all_gather x1, blocking collectives, shards(): lax.all_gather(keys, 'sp', axis=0, tiled=True)  6.73 us
    all_gather x1, blocking collectives, shards(): lax.all_gather(values, 'sp', axis=0, tiled=True)  5.59 us
  transfers between devices with their start and end apart: 3, of which 1 were waited for; matrix products, arithmetic and copies ran while one was open for 7% of the time, Pallas kernels for 0%

commit v1 on v0

--- a/solution.py
+++ b/solution.py
@@ -1,16 +1,320 @@
+import functools
 import math
 
 import jax
 import jax.numpy as jnp
 from jax import lax
+from jax.experimental import pallas as pl
+from jax.experimental.pallas import tpu as pltpu
 from jax.sharding import PartitionSpec as P
 
 HEADS = 12
 KV_HEADS = 2
 HEAD_DIM = 256
-
-
-def shards(queries, attn_out, log_norm, cotangent, keys, values, source, w_query, w_key, w_value):
+CORES = 2
+SIDE = 2
+VMEM_BYTES = 60 * 1024 * 1024
+MESH = pl.DeviceIdType.MESH
+NT = (((1,), (1,)), ((), ()))
+TN = (((0,), (0,)), ((), ()))
+F32 = jnp.float32
+BF16 = jnp.bfloat16
+
+
+def dot(a, b, dims=(((1,), (0,)), ((), ()))):
+    return lax.dot_general(a, b, dims, preferred_element_type=F32)
+
+
+def kernel(
+    sp, tp, lse_ref, k_ref, v_ref, q_hbm, o_hbm, do_hbm, src_hbm, wq_hbm, wk_hbm, wv_hbm,
+    dt_ref, ds_ref, dw_ref,
+    kv, qs, dos, os_, wq, wk, wv, src, lse, delta, dqa, dq16, part, got, full,
+    load_sem, near_send, near_recv, kv_send, kv_recv, kv_pair_send, kv_pair_recv,
+    src_send, src_recv, part_send, part_recv, g_send, g_recv, gy_send, gy_recv, gp_send, gp_recv,
+):
+    rows = q_hbm.shape[0]
+    rs, kw = k_ref.shape
+    repeat = HEADS // KV_HEADS
+    scale = 1.0 / math.sqrt(HEAD_DIM)
+    i, j = lax.axis_index("sp"), lax.axis_index("tp")
+    ny, nz = sp // CORES, tp // SIDE
+    y, c = i // CORES, lax.rem(i, CORES)
+    z, x = j // SIDE, lax.rem(j, SIDE)
+    sp_peers = [lax.rem(i + k, sp) for k in range(1, sp)]
+    y_peers = [lax.rem(y + k, ny) * CORES + c for k in range(1, ny)]
+    pair = y * CORES + 1 - c
+    zs = [lax.rem(z + k, nz) for k in range(1, nz)]
+    z_peers = [a * SIDE + x for a in zs]
+    jx = z * SIDE + 1 - x
+    sends = []
+
+    def send(ref_from, ref_to, s, r, device):
+        copy = pltpu.make_async_remote_copy(
+            src_ref=ref_from, dst_ref=ref_to, send_sem=s, recv_sem=r,
+            device_id=device, device_id_type=MESH,
+        )
+        copy.start()
+        sends.append(copy)
+
+    def receive(ref, r):
+        pltpu.make_async_remote_copy(
+            src_ref=ref, dst_ref=ref, send_sem=load_sem.at[0], recv_sem=r,
+            device_id=(pair, j), device_id_type=MESH,
+        ).wait_recv()
+
+    loads = []
+
+    def load(ref_from, ref_to):
+        copy = pltpu.make_async_copy(ref_from, ref_to, load_sem.at[len(loads)])
+        copy.start()
+        loads.append(copy)
+        return copy
+
+    barrier = pltpu.get_barrier_semaphore()
+    near = [(p, j) for p in sp_peers] + [(i, p) for p in z_peers] + [(i, jx)]
+    for d in near:
+        pl.semaphore_signal(barrier, inc=1, device_id=d, device_id_type=MESH)
+    near_rows = pl.ds(pl.multiple_of(i * rs, rs), rs)
+    own_copies = [load(r, kv.at[t, j, near_rows]) for t, r in enumerate((k_ref, v_ref))]
+    attn_loads = []
+    for g in range(KV_HEADS):
+        for h in range(repeat):
+            columns = pl.ds((g * repeat + h) * HEAD_DIM, HEAD_DIM)
+            for a, b in ((q_hbm, qs), (do_hbm, dos), (o_hbm, os_)):
+                attn_loads.append(load(a.at[:, columns], b.at[g, pl.ds(h * rows, rows)]))
+    src_load = load(src_hbm, src.at[i])
+    weight_loads = [load(wq_hbm, wq), load(wk_hbm, wk), load(wv_hbm, wv)]
+    pl.semaphore_wait(barrier, len(near))
+
+    for n, p in enumerate(sp_peers):
+        for t, r in enumerate((k_ref, v_ref)):
+            send(r, kv.at[t, j, near_rows], near_send.at[t, n], near_recv.at[t, i], (p, j))
+
+    src_load.wait()
+    for n, p in enumerate(y_peers):
+        send(src.at[i], src.at[i], src_send.at[n], src_recv.at[i], (p, j))
+    send(src.at[i], src.at[i], src_send.at[ny], src_recv.at[i], (pair, j))
+
+    for copy in attn_loads:
+        copy.wait()
+    for g in range(KV_HEADS):
+        for h in range(repeat):
+            at = pl.ds(h * rows, rows)
+            d = jnp.sum(dos[g, at].astype(F32) * os_[g, at].astype(F32), axis=1, keepdims=True)
+            delta[g, at] = jnp.broadcast_to(d, (rows, 128))
+            n = g * repeat + h
+            lse[g, at] = jnp.broadcast_to(lse_ref[:, n:n + 1], (rows, 128))
+
+    for copy in own_copies:
+        copy.wait()
+    for p in sp_peers:
+        for t in range(2):
+            receive(kv.at[t, j, pl.ds(pl.multiple_of(p * rs, rs), rs)], near_recv.at[t, p])
+
+    def kv_to_x(slot, n):
+        send(kv.at[c, slot], kv.at[c, slot], kv_send.at[n], kv_recv.at[slot], (i, jx))
+
+    def kv_to_pair(slot):
+        send(kv.at[c, slot], kv.at[c, slot], kv_pair_send.at[slot], kv_pair_recv.at[slot], (pair, j))
+
+    kv_to_x(j, 0)
+    for n, p in enumerate(z_peers):
+        send(kv.at[c, j], kv.at[c, j], kv_send.at[nz + n], kv_recv.at[j], (i, p))
+
+    def wide(a, n):
+        return a if n == 1 else jnp.concatenate([a] * n, axis=1)
+
+    def grads(g, keys, values):
+        n = keys.shape[0] // 128
+        p = jnp.exp(dot(qs[g], keys, NT) * scale - wide(lse[g], n))
+        dp = dot(dos[g], values, NT)
+        ds = (p * (dp - wide(delta[g], n))).astype(BF16)
+        return p, ds
+
+    def head_columns(g):
+        return slice(g * HEAD_DIM, (g + 1) * HEAD_DIM)
+
+    for g in range(KV_HEADS):
+        cols = head_columns(g)
+        keys = kv[0, j, :, cols]
+        p, ds = grads(g, keys, kv[1, j, :, cols])
+        dk = dot(ds, qs[g], TN) * scale
+        dv = dot(p.astype(BF16), dos[g], TN)
+        part[:, 0, :, cols] = dk.astype(BF16).reshape(sp, rs, HEAD_DIM)
+        part[:, 1, :, cols] = dv.astype(BF16).reshape(sp, rs, HEAD_DIM)
+        dqa[g] = dot(ds, keys)
+    for n, p in enumerate(sp_peers):
+        send(part.at[p], got.at[i], part_send.at[n], part_recv.at[i], (p, j))
+
+    def chunk_one(slot):
+        for g in range(KV_HEADS):
+            cols = head_columns(g)
+            keys = kv[0, slot, :, cols]
+            _, ds = grads(g, keys, kv[1, slot, :, cols])
+            dqa[g] += dot(ds, keys)
+
+    def chunk_z(a):
+        slots = pl.ds(a * SIDE, SIDE)
+        for g in range(KV_HEADS):
+            cols = head_columns(g)
+            keys = kv[0, slots, :, cols].reshape(-1, HEAD_DIM)
+            values = kv[1, slots, :, cols].reshape(-1, HEAD_DIM)
+            _, ds = grads(g, keys, values)
+            dqa[g] += dot(ds, keys)
+
+    def from_z(n):
+        slot = z_peers[n]
+        receive(kv.at[c, slot], kv_recv.at[slot])
+        kv_to_x(slot, n + 1)
+        kv_to_pair(slot)
+
+    def from_x(slot):
+        receive(kv.at[c, slot], kv_recv.at[slot])
+        kv_to_pair(slot)
+
+    def from_pair(slot):
+        receive(kv.at[1 - c, slot], kv_pair_recv.at[slot])
+
+    def g_to_x(slot, n):
+        send(full.at[i, slot], full.at[i, slot], g_send.at[n], g_recv.at[slot], (i, jx))
+
+    def g_spread(slot):
+        for n, p in enumerate(y_peers):
+            send(full.at[i, slot, 1], full.at[i, slot, 1], gy_send.at[n, slot], gy_recv.at[i, slot], (p, j))
+        send(full.at[i, slot, 1], full.at[i, slot, 1], gp_send.at[i, slot], gp_recv.at[i, slot], (pair, j))
+
+    def g_from_z(n):
+        slot = z_peers[n]
+        receive(full.at[i, slot], g_recv.at[slot])
+        g_to_x(slot, n + 1)
+        g_spread(slot)
+
+    def g_from_x(slot):
+        receive(full.at[i, slot], g_recv.at[slot])
+        g_spread(slot)
+
+    def g_from_y(slot):
+        for p in y_peers:
+            receive(full.at[p, slot, 1], gy_recv.at[p, slot])
+            send(full.at[p, slot, 1], full.at[p, slot, 1], gp_send.at[p, slot], gp_recv.at[p, slot], (pair, j))
+
+    from_x(jx)
+    from_z(0)
+    for n, p in enumerate(y_peers):
+        receive(src.at[p], src_recv.at[p])
+        send(src.at[p], src.at[p], src_send.at[ny + 1 + n], src_recv.at[p], (pair, j))
+    from_pair(jx)
+    chunk_one(jx)
+
+    total = part[i].astype(F32)
+    for p in sp_peers:
+        receive(got.at[p], part_recv.at[p])
+        total += got[p].astype(F32)
+    full[i, j] = total.astype(BF16)
+    for n in range(1, nz - 2):
+        from_z(n)
+    g_to_x(j, 0)
+    for n, p in enumerate(z_peers):
+        send(full.at[i, j], full.at[i, j], g_send.at[nz + n], g_recv.at[j], (i, p))
+    g_spread(j)
+    far = [a * SIDE + 1 - x for a in zs]
+    from_x(far[0])
+    from_pair(z_peers[0])
+    from_pair(far[0])
+    chunk_z(zs[0])
+    for n in range(nz - 1):
+        if n == 1:
+            from_z(nz - 2)
+            from_x(far[1])
+            from_pair(z_peers[1])
+            from_pair(far[1])
+            chunk_z(zs[1])
+        g_from_z(n)
+        if n == 0:
+            g_from_x(jx)
+            g_from_y(j)
+    for n in range(2, nz - 1):
+        from_x(far[n])
+        from_pair(z_peers[n])
+        from_pair(far[n])
+        chunk_z(zs[n])
+    for n in range(nz - 1):
+        g_from_x(far[n])
+    for copy in weight_loads:
+        copy.wait()
+    for g in range(KV_HEADS):
+        for h in range(repeat):
+            n = g * repeat + h
+            dq16[:, n * HEAD_DIM:(n + 1) * HEAD_DIM] = (dqa[g, h * rows:(h + 1) * rows] * scale).astype(BF16)
+    dt_ref[...] = dot(dq16[...], wq[...], NT).astype(BF16)
+    for slot in [jx] + z_peers + far:
+        g_from_y(slot)
+    ds_ref[...] = (
+        dot(full[i, :, 0].reshape(-1, kw), wk[...], NT) + dot(full[i, :, 1].reshape(-1, kw), wv[...], NT)
+    ).astype(BF16)
+    theirs = [lax.rem(y + k, ny) * CORES + 1 - c for k in range(ny)]
+    for p in theirs:
+        receive(src.at[p], src_recv.at[p])
+        for slot in range(tp):
+            receive(full.at[p, slot, 1], gp_recv.at[p, slot])
+    dw = dot(src[0], full[0, :, 1].reshape(-1, kw), TN)
+    for b in range(1, sp):
+        dw += dot(src[b], full[b, :, 1].reshape(-1, kw), TN)
+    dw_ref[...] = dw
+    for copy in sends:
+        copy.wait_send()
+
+
+def fused(sp, tp, scratch, queries, attn_out, log_norm, cotangent, keys, values, source, w_query, w_key, w_value):
+    rows = queries.shape[0]
+    width = w_value.shape[0]
+    vmem, hbm = pl.BlockSpec(memory_space=pltpu.VMEM), pl.BlockSpec(memory_space=pl.ANY)
+    dma = pltpu.SemaphoreType.DMA
+    nz, ny = tp // SIDE, sp // CORES
+    return pl.pallas_call(
+        functools.partial(kernel, sp, tp),
+        out_shape=(
+            jax.ShapeDtypeStruct((rows, width), BF16),
+            jax.ShapeDtypeStruct((source.shape[0], width), BF16),
+            jax.ShapeDtypeStruct(w_value.shape, F32),
+        ),
+        in_specs=[vmem] * 3 + [hbm] * 7,
+        out_specs=(vmem,) * 3,
+        scratch_shapes=[pltpu.VMEM(s, t) for s, t in scratch] + [
+            dma((3 * HEADS + 6,)), dma((2, sp)), dma((2, sp)), dma((2 * nz,)), dma((tp,)), dma((tp,)), dma((tp,)),
+            dma((2 * ny,)), dma((sp,)), dma((sp,)), dma((sp,)), dma((2 * nz,)), dma((tp,)),
+            dma((ny, tp)), dma((sp, tp)), dma((sp, tp)), dma((sp, tp)),
+        ],
+        compiler_params=pltpu.CompilerParams(
+            collective_id=0, has_side_effects=True, vmem_limit_bytes=VMEM_BYTES
+        ),
+    )(log_norm, keys, values, queries, attn_out, cotangent, source, w_query, w_key, w_value)
+
+
+def scratch_of(sp, tp, queries, keys, source, w_query, w_value):
+    rows, width = queries.shape
+    rs, kw = keys.shape
+    stack = (KV_HEADS, rows * HEADS // KV_HEADS, HEAD_DIM)
+    flat = stack[:2] + (128,)
+    return [
+        ((2, tp, sp * rs, kw), BF16), (stack, BF16), (stack, BF16), (stack, BF16),
+        (w_query.shape, BF16), (w_value.shape, BF16), (w_value.shape, BF16),
+        ((sp,) + source.shape, BF16), (flat, F32), (flat, F32), (stack, F32), ((rows, width), BF16),
+        ((sp, 2, rs, kw), BF16), ((sp, 2, rs, kw), BF16), ((sp, tp, 2, rs, kw), BF16),
+    ]
+
+
+def shards(sp, tp, *args):
+    queries, _, _, _, keys, _, source, w_query, _, w_value = args
+    scratch = scratch_of(sp, tp, queries, keys, source, w_query, w_value)
+    size = sum(math.prod(s) * jnp.dtype(t).itemsize for s, t in scratch)
+    fits = size * 2 < VMEM_BYTES and sp * keys.shape[0] == 128
+    if fits and sp % CORES == 0 and tp == 4 * SIDE:
+        return fused(sp, tp, scratch, *args)
+    return plain(*args)
+
+
+def plain(queries, attn_out, log_norm, cotangent, keys, values, source, w_query, w_key, w_value):
     single_precision = jnp.float32
     repeat = HEADS // KV_HEADS
     score_scale = 1.0 / math.sqrt(HEAD_DIM)
@@ -105,6 +409,7 @@
 
 
 def solution(mesh):
+    body = functools.partial(shards, mesh.shape["sp"], mesh.shape["tp"])
     in_specs = (
         P("sp", None),
         P("sp", None),
@@ -118,4 +423,4 @@
         P("tp", None),
     )
     out_specs = (P("sp", "tp"), P("sp", "tp"), P("tp", None))
-    return jax.shard_map(shards, mesh=mesh, in_specs=in_specs, out_specs=out_specs, check_vma=False)
+    return jax.shard_map(body, mesh=mesh, in_specs=in_specs, out_specs=out_specs, check_vma=False)

time: 198 us -> 53.9 us (0.27)
  blocking collectives: 125 us -> 0 us
  Pallas kernels: 0 us -> 46.3 us
  waiting for transfers between devices: 31.6 us -> 0 us
  between operations: 13.9 us -> 0.64 us
  matrix products: 8.94 us -> 0 us
  local copies, waits for them, and re-layouts: 15.6 us -> 6.66 us
  other arithmetic: 2.26 us -> 0 us
    psum x1 -> x0, blocking collectives: 80.8 us -> none  [shards(): dq16 = lax.psum(query_gradient_piece, 'tp').astype(jnp.bfloat16)]
    pallas_call x0 -> x1, Pallas kernels: none -> 46.3 us  [fused(): pl.pallas_call(functools.partial(kernel, sp, tp), out_shape=(jax.ShapeDty...]
    all_gather x3 -> x0, blocking collectives: 43.8 us -> none  [the longest x1 31.5 us: shards(): group = lax.all_gather(stacked, 'tp', axis=0, tiled=True)]
    psum x1 -> x0, waiting for transfers between devices: 31.5 us -> none  [shards(): lax.psum(weight_term.astype(jnp.bfloat16), 'sp').astype(jnp.float32)]
    dot_general x8 -> x0, matrix products: 8.94 us -> none  [the longest x1 2.25 us: shards(): lax.dot_general(group, weights, (((1,), (1,)), ((), ())), preferred_eleme...]
    unnamed x24 -> x4, local copies, waits for them, and re-layouts: 10.6 us -> 6.66 us
    mul x1 -> x0, local copies, waits for them, and re-layouts: 3.03 us -> none  [shards(): jnp.einsum('wohn,nwb->hwob', score_gradient, shared_key_heads, preferred_...]
  transfers between devices with their start and end apart: 3 -> 0, of which waited for: 1 -> 0; matrix products, arithmetic and copies ran while one was open for 7% -> 0% of each run, Pallas kernels for 0% -> 0%
where the time goes in v1:
time: 53.9 us; the launch traced here: 53.6 us
  Pallas kernels  46.3 us (86%)
  local copies, waits for them, and re-layouts  6.66 us (12%)
  between operations  0.64 us (1%)
    pallas_call x1, Pallas kernels, fused(): pl.pallas_call(functools.partial(kernel, sp, tp), out_shape=(jax.ShapeDty...  46.3 us
    unnamed x4, local copies, waits for them, and re-layouts  6.66 us

profile of v1, /device:TPU:0, one launch (start us, length us, event | category | flops | bytes accessed | tf_op | source)
XLA Modules:
  0.0 53.6 jit_solution(15195582912277386415)
XLA Ops:
  0.6 1.4 %copy.13.lse_ref = f32[128,12]{1,0:T(8,128)} copy(f32[128,12]{0,1:T(8,128)} %param.12) | data formatting | bytes 12288 | tf_op args[2]
  2.1 46.3 %shard_map.121 = (bf16[128,384]{1,0:T(8,128)(2,1)}, bf16[256,384]{1,0:T(8,128)(2,1)}, f32[384,512]{1,0:T(8,128)}) custom-call(f32[128,12]{1,0:T(8,128)} %copy.13.lse_ref, bf16[32,512]{1,0:T(8,128)(2,1)} %k_ref.1, bf16[32,512]{1,0:T(8,128)(2,1)} %v_ref.1, bf16[128,3072]{1,0:T(8,128)(2,1)} %q_hbm.1, bf16[128,3072]{1,0:T(8,128)(2,1)} %o_hbm.1, ...), custom_call_target="tpu_custom_call" | custom-call | tf_op jit(solution)/shard_map/pallas_call | solution.py:274
  48.3 1.5 %copy.17 = bf16[128,384]{1,0:T(8,128)(2,1)} copy(bf16[128,384]{1,0:T(8,128)(2,1)} %get-tuple-element.6) | data formatting | bytes 196608
  49.9 1.6 %copy.18 = bf16[256,384]{1,0:T(8,128)(2,1)} copy(bf16[256,384]{1,0:T(8,128)(2,1)} %get-tuple-element.7) | data formatting | bytes 393216
  51.5 2.1 %copy.19 = f32[384,512]{1,0:T(8,128)} copy(f32[384,512]{1,0:T(8,128)} %get-tuple-element.8) | data formatting | bytes 1572864

commit v2 on v1

--- a/solution.py
+++ b/solution.py
@@ -27,10 +27,10 @@
 
 def kernel(
     sp, tp, lse_ref, k_ref, v_ref, q_hbm, o_hbm, do_hbm, src_hbm, wq_hbm, wk_hbm, wv_hbm,
-    dt_ref, ds_ref, dw_ref,
-    kv, qs, dos, os_, wq, wk, wv, src, lse, delta, dqa, dq16, part, got, full,
+    dt_hbm, ds_hbm, dw_hbm,
+    dt_ref, ds_ref, dw_ref, kv, qs, dos, os_, wq, wk, wv, src, src_t, lse, delta, dqa, dq16, part, got, full,
     load_sem, near_send, near_recv, kv_send, kv_recv, kv_pair_send, kv_pair_recv,
-    src_send, src_recv, part_send, part_recv, g_send, g_recv, gy_send, gy_recv, gp_send, gp_recv,
+    src_send, src_recv, part_send, part_recv, g_send, g_recv, gy_send, gy_recv, gp_send, gp_recv, kvz_send, gz_send,
 ):
     rows = q_hbm.shape[0]
     rs, kw = k_ref.shape
@@ -43,10 +43,26 @@
     sp_peers = [lax.rem(i + k, sp) for k in range(1, sp)]
     y_peers = [lax.rem(y + k, ny) * CORES + c for k in range(1, ny)]
     pair = y * CORES + 1 - c
-    zs = [lax.rem(z + k, nz) for k in range(1, nz)]
+    orders = [sorted((b for b in range(nz) if b != a), key=lambda b, a=a: abs(a - b)) for a in range(nz)]
+    zs = [sum(jnp.where(z == a, order[n], 0) for a, order in enumerate(orders)) for n in range(nz - 1)]
+    onward = [jnp.where(a > z, z - 1, z + 1) for a in zs]
+    onward_ok = [(b >= 0) & (b < nz) for b in onward]
     z_peers = [a * SIDE + x for a in zs]
     jx = z * SIDE + 1 - x
     sends = []
+    maybe_sends = []
+
+    def send_if(condition, make):
+        pl.when(condition)(lambda: make().start())
+        maybe_sends.append((condition, make))
+
+    def along_z(ref, n, s, r):
+        targets = [(z + 1, z + 1 < nz, 0), (z - 1, z >= 1, 1)] if n is None else [(onward[n], onward_ok[n], n + 2)]
+        for to, ok, at in targets:
+            send_if(ok, lambda to=to, at=at: pltpu.make_async_remote_copy(
+                src_ref=ref, dst_ref=ref, send_sem=s.at[at], recv_sem=r,
+                device_id=(i, to * SIDE + x), device_id_type=MESH,
+            ))
 
     def send(ref_from, ref_to, s, r, device):
         copy = pltpu.make_async_remote_copy(
@@ -90,11 +106,6 @@
         for t, r in enumerate((k_ref, v_ref)):
             send(r, kv.at[t, j, near_rows], near_send.at[t, n], near_recv.at[t, i], (p, j))
 
-    src_load.wait()
-    for n, p in enumerate(y_peers):
-        send(src.at[i], src.at[i], src_send.at[n], src_recv.at[i], (p, j))
-    send(src.at[i], src.at[i], src_send.at[ny], src_recv.at[i], (pair, j))
-
     for copy in attn_loads:
         copy.wait()
     for g in range(KV_HEADS):
@@ -103,7 +114,7 @@
             d = jnp.sum(dos[g, at].astype(F32) * os_[g, at].astype(F32), axis=1, keepdims=True)
             delta[g, at] = jnp.broadcast_to(d, (rows, 128))
             n = g * repeat + h
-            lse[g, at] = jnp.broadcast_to(lse_ref[:, n:n + 1], (rows, 128))
+            lse[g, at] = jnp.transpose(jnp.broadcast_to(lse_ref[n:n + 1, :], (128, rows)))
 
     for copy in own_copies:
         copy.wait()
@@ -118,8 +129,7 @@
         send(kv.at[c, slot], kv.at[c, slot], kv_pair_send.at[slot], kv_pair_recv.at[slot], (pair, j))
 
     kv_to_x(j, 0)
-    for n, p in enumerate(z_peers):
-        send(kv.at[c, j], kv.at[c, j], kv_send.at[nz + n], kv_recv.at[j], (i, p))
+    along_z(kv.at[c, j], None, kvz_send, kv_recv.at[j])
 
     def wide(a, n):
         return a if n == 1 else jnp.concatenate([a] * n, axis=1)
@@ -145,6 +155,10 @@
         dqa[g] = dot(ds, keys)
     for n, p in enumerate(sp_peers):
         send(part.at[p], got.at[i], part_send.at[n], part_recv.at[i], (p, j))
+    src_load.wait()
+    for n, p in enumerate(y_peers):
+        send(src.at[i], src.at[i], src_send.at[n], src_recv.at[i], (p, j))
+    send(src.at[i], src.at[i], src_send.at[ny], src_recv.at[i], (pair, j))
 
     def chunk_one(slot):
         for g in range(KV_HEADS):
@@ -165,6 +179,7 @@
     def from_z(n):
         slot = z_peers[n]
         receive(kv.at[c, slot], kv_recv.at[slot])
+        along_z(kv.at[c, slot], n, kvz_send, kv_recv.at[slot])
         kv_to_x(slot, n + 1)
         kv_to_pair(slot)
 
@@ -186,6 +201,7 @@
     def g_from_z(n):
         slot = z_peers[n]
         receive(full.at[i, slot], g_recv.at[slot])
+        along_z(full.at[i, slot], n, gz_send, g_recv.at[slot])
         g_to_x(slot, n + 1)
         g_spread(slot)
 
@@ -198,71 +214,107 @@
             receive(full.at[p, slot, 1], gy_recv.at[p, slot])
             send(full.at[p, slot, 1], full.at[p, slot, 1], gp_send.at[p, slot], gp_recv.at[p, slot], (pair, j))
 
+    far = [a * SIDE + 1 - x for a in zs]
     from_x(jx)
     from_z(0)
-    for n, p in enumerate(y_peers):
-        receive(src.at[p], src_recv.at[p])
-        send(src.at[p], src.at[p], src_send.at[ny + 1 + n], src_recv.at[p], (pair, j))
-    from_pair(jx)
-    chunk_one(jx)
-
     total = part[i].astype(F32)
     for p in sp_peers:
         receive(got.at[p], part_recv.at[p])
         total += got[p].astype(F32)
     full[i, j] = total.astype(BF16)
-    for n in range(1, nz - 2):
-        from_z(n)
+    along_z(full.at[i, j], None, gz_send, g_recv.at[j])
     g_to_x(j, 0)
-    for n, p in enumerate(z_peers):
-        send(full.at[i, j], full.at[i, j], g_send.at[nz + n], g_recv.at[j], (i, p))
     g_spread(j)
-    far = [a * SIDE + 1 - x for a in zs]
-    from_x(far[0])
-    from_pair(z_peers[0])
-    from_pair(far[0])
-    chunk_z(zs[0])
+    from_pair(jx)
+    chunk_one(jx)
     for n in range(nz - 1):
-        if n == 1:
-            from_z(nz - 2)
-            from_x(far[1])
-            from_pair(z_peers[1])
-            from_pair(far[1])
-            chunk_z(zs[1])
+        if n + 1 < nz - 1:
+            from_z(n + 1)
+        from_x(far[n])
         g_from_z(n)
         if n == 0:
             g_from_x(jx)
-            g_from_y(j)
-    for n in range(2, nz - 1):
-        from_x(far[n])
+            for m, p in enumerate(y_peers):
+                receive(src.at[p], src_recv.at[p])
+                send(src.at[p], src.at[p], src_send.at[ny + 1 + m], src_recv.at[p], (pair, j))
+        else:
+            g_from_x(far[n - 1])
+        g_from_y([j, jx, z_peers[0]][n])
         from_pair(z_peers[n])
         from_pair(far[n])
         chunk_z(zs[n])
-    for n in range(nz - 1):
-        g_from_x(far[n])
+    g_from_x(far[nz - 2])
     for copy in weight_loads:
         copy.wait()
     for g in range(KV_HEADS):
         for h in range(repeat):
             n = g * repeat + h
             dq16[:, n * HEAD_DIM:(n + 1) * HEAD_DIM] = (dqa[g, h * rows:(h + 1) * rows] * scale).astype(BF16)
+    theirs = [lax.rem(y + k, ny) * CORES + 1 - c for k in range(ny)]
+    for p in theirs:
+        receive(src.at[p], src_recv.at[p])
+    for b in range(sp):
+        src_t[b] = jnp.transpose(src[b])
     dt_ref[...] = dot(dq16[...], wq[...], NT).astype(BF16)
-    for slot in [jx] + z_peers + far:
+    results = [load(dt_ref, dt_hbm)]
+    for slot in z_peers[1:] + far:
         g_from_y(slot)
     ds_ref[...] = (
         dot(full[i, :, 0].reshape(-1, kw), wk[...], NT) + dot(full[i, :, 1].reshape(-1, kw), wv[...], NT)
     ).astype(BF16)
-    theirs = [lax.rem(y + k, ny) * CORES + 1 - c for k in range(ny)]
+    results.append(load(ds_ref, ds_hbm))
     for p in theirs:
-        receive(src.at[p], src_recv.at[p])
         for slot in range(tp):
             receive(full.at[p, slot, 1], gp_recv.at[p, slot])
-    dw = dot(src[0], full[0, :, 1].reshape(-1, kw), TN)
+    dw = dot(src_t[0], full[0, :, 1].reshape(-1, kw))
     for b in range(1, sp):
-        dw += dot(src[b], full[b, :, 1].reshape(-1, kw), TN)
+        dw += dot(src_t[b], full[b, :, 1].reshape(-1, kw))
     dw_ref[...] = dw
+    results.append(load(dw_ref, dw_hbm))
+    for copy in results:
+        copy.wait()
     for copy in sends:
         copy.wait_send()
+    for condition, make in maybe_sends:
+        pl.when(condition)(lambda make=make: make().wait_send())
+
+
+def settle(*refs):
+    count = (len(refs) - 1) // 3
+    sems = refs[-1]
+    ins, outs, held = (refs[n * count:(n + 1) * count] for n in range(3))
+    steps = []
+    for n in range(count):
+        tall = ins[n].shape[0]
+        pieces = 4 if n == count - 1 and tall % 32 == 0 else 1
+        for m in range(pieces):
+            at = pl.ds(m * (tall // pieces), tall // pieces)
+            k = len(steps)
+            steps.append((
+                pltpu.make_async_copy(ins[n].at[at], held[n].at[at], sems.at[0, k]),
+                pltpu.make_async_copy(held[n].at[at], outs[n].at[at], sems.at[1, k]),
+            ))
+    for arrive, _ in steps:
+        arrive.start()
+    for arrive, leave in steps:
+        arrive.wait()
+        leave.start()
+    for _, leave in steps:
+        leave.wait()
+
+
+def settled(arrays):
+    hbm = pl.BlockSpec(memory_space=pl.ANY)
+    return pl.pallas_call(
+        settle,
+        out_shape=tuple(jax.ShapeDtypeStruct(a.shape, a.dtype) for a in arrays),
+        in_specs=[hbm] * len(arrays),
+        out_specs=(hbm,) * len(arrays),
+        scratch_shapes=[pltpu.VMEM(a.shape, a.dtype) for a in arrays] + [
+            pltpu.SemaphoreType.DMA((2, len(arrays) + 3))
+        ],
+        compiler_params=pltpu.CompilerParams(vmem_limit_bytes=VMEM_BYTES),
+    )(*arrays)
 
 
 def fused(sp, tp, scratch, queries, attn_out, log_norm, cotangent, keys, values, source, w_query, w_key, w_value):
@@ -271,7 +323,7 @@
     vmem, hbm = pl.BlockSpec(memory_space=pltpu.VMEM), pl.BlockSpec(memory_space=pl.ANY)
     dma = pltpu.SemaphoreType.DMA
     nz, ny = tp // SIDE, sp // CORES
-    return pl.pallas_call(
+    return settled(pl.pallas_call(
         functools.partial(kernel, sp, tp),
         out_shape=(
             jax.ShapeDtypeStruct((rows, width), BF16),
@@ -279,16 +331,18 @@
             jax.ShapeDtypeStruct(w_value.shape, F32),
         ),
         in_specs=[vmem] * 3 + [hbm] * 7,
-        out_specs=(vmem,) * 3,
-        scratch_shapes=[pltpu.VMEM(s, t) for s, t in scratch] + [
-            dma((3 * HEADS + 6,)), dma((2, sp)), dma((2, sp)), dma((2 * nz,)), dma((tp,)), dma((tp,)), dma((tp,)),
+        out_specs=(hbm,) * 3,
+        scratch_shapes=[
+            pltpu.VMEM((rows, width), BF16), pltpu.VMEM((source.shape[0], width), BF16), pltpu.VMEM(w_value.shape, F32),
+        ] + [pltpu.VMEM(s, t) for s, t in scratch] + [
+            dma((3 * HEADS + 9,)), dma((2, sp)), dma((2, sp)), dma((2 * nz,)), dma((tp,)), dma((tp,)), dma((tp,)),
             dma((2 * ny,)), dma((sp,)), dma((sp,)), dma((sp,)), dma((2 * nz,)), dma((tp,)),
-            dma((ny, tp)), dma((sp, tp)), dma((sp, tp)), dma((sp, tp)),
+            dma((ny, tp)), dma((sp, tp)), dma((sp, tp)), dma((sp, tp)), dma((nz + 1,)), dma((nz + 1,)),
         ],
         compiler_params=pltpu.CompilerParams(
             collective_id=0, has_side_effects=True, vmem_limit_bytes=VMEM_BYTES
         ),
-    )(log_norm, keys, values, queries, attn_out, cotangent, source, w_query, w_key, w_value)
+    )(log_norm.T, keys, values, queries, attn_out, cotangent, source, w_query, w_key, w_value))
 
 
 def scratch_of(sp, tp, queries, keys, source, w_query, w_value):
@@ -299,7 +353,7 @@
     return [
         ((2, tp, sp * rs, kw), BF16), (stack, BF16), (stack, BF16), (stack, BF16),
         (w_query.shape, BF16), (w_value.shape, BF16), (w_value.shape, BF16),
-        ((sp,) + source.shape, BF16), (flat, F32), (flat, F32), (stack, F32), ((rows, width), BF16),
+        ((sp,) + source.shape, BF16), ((sp,) + source.shape[::-1], BF16), (flat, F32), (flat, F32), (stack, F32), ((rows, width), BF16),
         ((sp, 2, rs, kw), BF16), ((sp, 2, rs, kw), BF16), ((sp, tp, 2, rs, kw), BF16),
     ]
 

time: 53.9 us -> 46.1 us (0.86)
  local copies, waits for them, and re-layouts: 6.66 us -> 0 us
  Pallas kernels: 46.3 us -> 45.3 us
    unnamed x4 -> x0, local copies, waits for them, and re-layouts: 6.66 us -> none
    pallas_call x1, Pallas kernels: 46.3 us -> 43.2 us  [fused(): pl.pallas_call(functools.partial(kernel, sp, tp), out_shape=(jax.ShapeDty...]
    pallas_call x0 -> x1, Pallas kernels: none -> 2.11 us  [settled(): pl.pallas_call(settle, out_shape=tuple((jax.ShapeDtypeStruct(a.shape, a.d...]
where the time goes in v2:
time: 46.1 us; the launch traced here: 45.9 us
  Pallas kernels  45.3 us (98%)
  between operations  0.64 us (1%)
    pallas_call x1, Pallas kernels, fused(): pl.pallas_call(functools.partial(kernel, sp, tp), out_shape=(jax.ShapeDty...  43.2 us
    pallas_call x1, Pallas kernels, settled(): pl.pallas_call(settle, out_shape=tuple((jax.ShapeDtypeStruct(a.shape, a.d...  2.11 us

profile of v2, /device:TPU:0, one launch (start us, length us, event | category | flops | bytes accessed | tf_op | source)
XLA Modules:
  0.0 45.9 jit_solution(15166122662577182465)
XLA Ops:
  0.6 43.2 %shard_map.121 = (bf16[128,384]{1,0:T(8,128)(2,1)}, bf16[256,384]{1,0:T(8,128)(2,1)}, f32[384,512]{1,0:T(8,128)}) custom-call(f32[12,128]{1,0:T(8,128)} %bitcast.1, bf16[32,512]{1,0:T(8,128)(2,1)} %k_ref.1, bf16[32,512]{1,0:T(8,128)(2,1)} %v_ref.1, bf16[128,3072]{1,0:T(8,128)(2,1)} %q_hbm.1, bf16[128,3072]{1,0:T(8,128)(2,1)} %o_hbm.1, ...), custom_call_target="tpu_custom_call" | custom-call | tf_op jit(solution)/shard_map/pallas_call | solution.py:326
  43.8 2.1 %shard_map.122 = (bf16[128,384]{1,0:T(8,128)(2,1)}, bf16[256,384]{1,0:T(8,128)(2,1)}, f32[384,512]{1,0:T(8,128)}) custom-call(bf16[128,384]{1,0:T(8,128)(2,1)} %get-tuple-element.6.refs_0_, bf16[256,384]{1,0:T(8,128)(2,1)} %get-tuple-element.7.refs_1_, f32[384,512]{1,0:T(8,128)} %get-tuple-element.8.refs_2_), custom_call_target="tpu_custom_call" | custom-call | tf_op jit(solution)/shard_map/pallas_call | solution.py:308

commit v3 on v2

--- a/solution.py
+++ b/solution.py
@@ -155,10 +155,6 @@
         dqa[g] = dot(ds, keys)
     for n, p in enumerate(sp_peers):
         send(part.at[p], got.at[i], part_send.at[n], part_recv.at[i], (p, j))
-    src_load.wait()
-    for n, p in enumerate(y_peers):
-        send(src.at[i], src.at[i], src_send.at[n], src_recv.at[i], (p, j))
-    send(src.at[i], src.at[i], src_send.at[ny], src_recv.at[i], (pair, j))
 
     def chunk_one(slot):
         for g in range(KV_HEADS):
@@ -225,6 +221,10 @@
     along_z(full.at[i, j], None, gz_send, g_recv.at[j])
     g_to_x(j, 0)
     g_spread(j)
+    src_load.wait()
+    for n, p in enumerate(y_peers):
+        send(src.at[i], src.at[i], src_send.at[n], src_recv.at[i], (p, j))
+    send(src.at[i], src.at[i], src_send.at[ny], src_recv.at[i], (pair, j))
     from_pair(jx)
     chunk_one(jx)
     for n in range(nz - 1):
@@ -234,11 +234,12 @@
         g_from_z(n)
         if n == 0:
             g_from_x(jx)
+        else:
+            g_from_x(far[n - 1])
+        if n == 1:
             for m, p in enumerate(y_peers):
                 receive(src.at[p], src_recv.at[p])
                 send(src.at[p], src.at[p], src_send.at[ny + 1 + m], src_recv.at[p], (pair, j))
-        else:
-            g_from_x(far[n - 1])
         g_from_y([j, jx, z_peers[0]][n])
         from_pair(z_peers[n])
         from_pair(far[n])

time: 46.1 us -> 46.1 us (level)
  no operation moved by 1% of the time
where the time goes in v3:
time: 46.1 us; the launch traced here: 45.9 us
  Pallas kernels  45.3 us (98%)
  between operations  0.64 us (1%)
    pallas_call x1, Pallas kernels, fused(): pl.pallas_call(functools.partial(kernel, sp, tp), out_shape=(jax.ShapeDty...  43.2 us
    pallas_call x1, Pallas kernels, settled(): pl.pallas_call(settle, out_shape=tuple((jax.ShapeDtypeStruct(a.shape, a.d...  2.11 us

profile of v3, /device:TPU:0, one launch (start us, length us, event | category | flops | bytes accessed | tf_op | source)
XLA Modules:
  0.0 45.9 jit_solution(1570241658915709630)
XLA Ops:
  0.6 43.2 %shard_map.121 = (bf16[128,384]{1,0:T(8,128)(2,1)}, bf16[256,384]{1,0:T(8,128)(2,1)}, f32[384,512]{1,0:T(8,128)}) custom-call(f32[12,128]{1,0:T(8,128)} %bitcast.1, bf16[32,512]{1,0:T(8,128)(2,1)} %k_ref.1, bf16[32,512]{1,0:T(8,128)(2,1)} %v_ref.1, bf16[128,3072]{1,0:T(8,128)(2,1)} %q_hbm.1, bf16[128,3072]{1,0:T(8,128)(2,1)} %o_hbm.1, ...), custom_call_target="tpu_custom_call" | custom-call | tf_op jit(solution)/shard_map/pallas_call | solution.py:327
  43.8 2.1 %shard_map.122 = (bf16[128,384]{1,0:T(8,128)(2,1)}, bf16[256,384]{1,0:T(8,128)(2,1)}, f32[384,512]{1,0:T(8,128)}) custom-call(bf16[128,384]{1,0:T(8,128)(2,1)} %get-tuple-element.6.refs_0_, bf16[256,384]{1,0:T(8,128)(2,1)} %get-tuple-element.7.refs_1_, f32[384,512]{1,0:T(8,128)} %get-tuple-element.8.refs_2_), custom_call_target="tpu_custom_call" | custom-call | tf_op jit(solution)/shard_map/pallas_call | solution.py:309
